TPU v7x, 32 devices: a whole 2x2x4 slice. The times are simulated.
32 devices in a mesh: sp: 8 (over z, x), dp: 4 (over y, core).
Axes of the slice: x: 2, y: 2, z: 4, core: 2. Of those that a mesh axis runs over, the one named last changes fastest.
Arguments:
- residual_in: bfloat16 [4, 1024, 2048], P('dp', 'sp'), may hold values from -6 to 6
- ssm_input: bfloat16 [4, 1024, 2048], P('dp', 'sp'), may hold values from -6 to 6
- state_b: bfloat16 [4, 1024, 2048], P('dp', 'sp'), may hold values from -6 to 6
- state_c: bfloat16 [4, 1024, 2048], P('dp', 'sp'), may hold values from -6 to 6
- step_raw: bfloat16 [4, 1024, 64], P('dp', 'sp'), may hold values from -4 to 3
- gate_input: bfloat16 [4, 1024, 2048], P('dp', 'sp'), may hold values from -6 to 6
- conv_x: float32 [7, 2048], P(None, 'sp'), may hold values from -2 to 2
- conv_b: float32 [7, 2048], P(None, 'sp'), may hold values from -2 to 2
- conv_c: float32 [7, 2048], P(None, 'sp'), may hold values from -2 to 2
- decay_rate: float32 [2, 32], P(None, 'sp'), may hold values from 0 to 1, as said below
- mix_gain: float32 [2048], replicated, may hold values from 0.1 to 1.9
- out_weight: bfloat16 [2048, 2048], P('dp'), may hold values from -0.125 to 0.125
- ffn_gain: float32 [2048], replicated, may hold values from 0.1 to 1.9
- routing: int32 [4, 1024, 4], P('dp', 'sp'), may hold values from 0 to 31, all different within a row; in each aligned block of 128 rows (0 to 127, 128 to 255, ..., all dimensions but the last counted through in order) at most 32 rows name the same one
- route_weight: float32 [4, 1024, 4], P('dp', 'sp'), may hold values from 0.1 to 0.6
- gate_w: bfloat16 [32, 2048, 1024], P(('sp', 'dp')), may hold values from -60 to 60
- up_w: bfloat16 [32, 2048, 1024], P(('sp', 'dp')), may hold values from -60 to 60
- down_w: bfloat16 [32, 1024, 2048], P(('sp', 'dp')), may hold values from -0.1875 to 0.1875
Outputs:
- block_out: bfloat16 [4, 1024, 2048], P('dp', 'sp')
Inputs may be any that keep to these rules, and one draw needn't show every extreme that they name: `routing`: each row names 4 different experts; within the rows of one device no expert is named by more than 32 rows, a bound that some block reaches. `decay_rate`: Positive.
All inputs are finite; a program needn't handle non-finite values.
Results may differ from a plain program's by a relative error of at most 0.0082.
Values may be sent and summed in bfloat16 or wider, within the bound.
No kernel may reach another device: no remote copies, remote signals or barrier semaphores. Data moves between devices by JAX's collectives and lax.ppermute only.
A program may use at most 128 MiB of HBM per device.

v0:
```python
import jax
import jax.numpy as jnp
from jax import lax
from jax.sharding import PartitionSpec as P

HEAD_DIM = 64
STATE = 128
BLOCK = 128
NORM_GROUPS = 4
highest = lax.Precision.HIGHEST
epsilon = 1e-05
clamp_limit = 7.0
sigmoid_slope = 1.702


def centred_conv(values, taps):
    half_width = taps.shape[0] // 2
    padded = jnp.pad(values, ((half_width, half_width), (0, 0)))
    total = jnp.zeros_like(values)
    for offset in range(taps.shape[0]):
        total = total + padded[offset : offset + values.shape[0]] * taps[offset]
    return total


def ssd_direction(signal, step_size, rates, write_map, read_map):
    length = signal.shape[0]
    head_count = signal.shape[1]
    head_width = signal.shape[2]
    group_count = write_map.shape[1]
    state_width = write_map.shape[2]
    per_group = head_count // group_count
    blocks = length // BLOCK
    scaled = (signal * step_size[..., None]).reshape(
        blocks, BLOCK, group_count, per_group, head_width
    )
    cumulative = jnp.cumsum(
        (-step_size * rates).reshape(blocks, BLOCK, group_count, per_group), axis=1
    )
    write_block = write_map.reshape(blocks, BLOCK, group_count, state_width)
    read_block = read_map.reshape(blocks, BLOCK, group_count, state_width)
    spread = cumulative[:, :, None] - cumulative[:, None]
    lower_mask = (lax.iota(jnp.int32, BLOCK)[:, None] >= lax.iota(jnp.int32, BLOCK)[None, :])[
        None, :, :, None, None
    ]
    weight_in = jnp.exp(jnp.where(lower_mask, spread, -jnp.inf))
    intersect = jnp.einsum("clgn,csgn->clsg", read_block, write_block, precision=highest)
    inside = jnp.einsum(
        "clsgk,csgkp->clgkp", intersect[..., None] * weight_in, scaled, precision=highest
    )
    to_end = jnp.exp(cumulative[:, -1:] - cumulative)
    states = jnp.einsum(
        "csgn,csgkp->cgkpn", write_block, scaled * to_end[..., None], precision=highest
    )
    carry_decay = jnp.exp(cumulative[:, -1])

    def advance(running, block_pair):
        block_state, factor = block_pair
        return (factor[..., None, None] * running + block_state, running)

    initial = jnp.zeros((group_count, per_group, head_width, state_width), jnp.float32)
    _, entering = lax.scan(advance, initial, (states, carry_decay))
    carried = (
        jnp.einsum("clgn,cgkpn->clgkp", read_block, entering, precision=highest)
        * jnp.exp(cumulative)[..., None]
    )
    return (inside + carried).reshape(length, head_count, head_width)


def both_ways(signal, steps_fwd, steps_bwd, rates, write_map, read_map):
    forward = ssd_direction(signal, steps_fwd, rates[0], write_map, read_map)
    backward = ssd_direction(
        jnp.flip(signal, 0),
        jnp.flip(steps_bwd, 0),
        rates[1],
        jnp.flip(write_map, 0),
        jnp.flip(read_map, 0),
    )
    return forward + jnp.flip(backward, 0)


def scale_rows(values, gains):
    return values * lax.rsqrt(jnp.mean(values * values, axis=-1, keepdims=True) + epsilon) * gains


def group_scale(values, gains):
    shaped = values.reshape(values.shape[:-1] + (NORM_GROUPS, values.shape[-1] // NORM_GROUPS))
    shaped = shaped * lax.rsqrt(jnp.mean(shaped * shaped, axis=-1, keepdims=True) + epsilon)
    return shaped.reshape(values.shape) * gains


def expert_apply(rows, gate_mat, up_mat, down_mat):
    gate_value = jnp.minimum(
        jnp.dot(rows, gate_mat, preferred_element_type=jnp.float32), clamp_limit
    )
    up_value = jnp.clip(
        jnp.dot(rows, up_mat, preferred_element_type=jnp.float32), -clamp_limit, clamp_limit
    )
    active = ((up_value + 1.0) * gate_value * jax.nn.sigmoid(sigmoid_slope * gate_value)).astype(
        jnp.bfloat16
    )
    return jnp.dot(active, down_mat, preferred_element_type=jnp.float32).astype(jnp.bfloat16)


def per_device(
    residual_in,
    ssm_input,
    state_b,
    state_c,
    step_raw,
    gate_input,
    conv_x,
    conv_b,
    conv_c,
    decay_rate,
    mix_gain,
    out_weight,
    ffn_gain,
    routing,
    route_weight,
    gate_w,
    up_w,
    down_w,
):
    signal_loc, write_loc, read_loc, step_loc = (
        lax.all_to_all(ssm_input, "sp", split_axis=2, concat_axis=1, tiled=True),
        lax.all_to_all(state_b, "sp", split_axis=2, concat_axis=1, tiled=True),
        lax.all_to_all(state_c, "sp", split_axis=2, concat_axis=1, tiled=True),
        lax.all_to_all(step_raw, "sp", split_axis=2, concat_axis=1, tiled=True),
    )
    length = signal_loc.shape[1]
    head_local = decay_rate.shape[1]
    signal = jax.nn.silu(centred_conv(signal_loc[0].astype(jnp.float32), conv_x)).reshape(
        length, head_local, HEAD_DIM
    )
    write_map = jax.nn.silu(centred_conv(write_loc[0].astype(jnp.float32), conv_b)).reshape(
        length, -1, STATE
    )
    read_map = jax.nn.silu(centred_conv(read_loc[0].astype(jnp.float32), conv_c)).reshape(
        length, -1, STATE
    )
    step_pair = jax.nn.softplus(step_loc[0].astype(jnp.float32).reshape(length, head_local, 2))
    mixed_heads = both_ways(
        signal, step_pair[..., 0], step_pair[..., 1], decay_rate, write_map, read_map
    )
    mixed_heads = mixed_heads.reshape(1, length, head_local * HEAD_DIM).astype(jnp.bfloat16)
    mixed_tokens = lax.all_to_all(mixed_heads, "sp", split_axis=1, concat_axis=2, tiled=True)
    token_count = residual_in.shape[1]
    model_width = residual_in.shape[2]
    gated = mixed_tokens[0].astype(jnp.float32) * jax.nn.silu(gate_input[0].astype(jnp.float32))
    mixed = group_scale(gated, mix_gain).astype(jnp.bfloat16)
    projected = jnp.dot(
        mixed,
        lax.all_gather(out_weight, "dp", axis=0, tiled=True),
        preferred_element_type=jnp.float32,
    )
    stream = residual_in[0].astype(jnp.float32) + projected
    ffn_input = scale_rows(stream, ffn_gain).astype(jnp.bfloat16)
    sp_count = lax.axis_size("sp")
    dp_count = lax.axis_size("dp")
    experts_all = sp_count * dp_count
    top_count = routing.shape[2]
    assigned = token_count * top_count
    capacity = 2 * assigned // experts_all
    flat_expert = routing.reshape(assigned)
    one_hot = (flat_expert[:, None] == lax.iota(jnp.int32, experts_all)[None, :]).astype(
        jnp.bfloat16
    )
    earlier = (
        lax.iota(jnp.int32, assigned)[:, None] > lax.iota(jnp.int32, assigned)[None, :]
    ).astype(jnp.bfloat16)
    before = jnp.dot(earlier, one_hot, preferred_element_type=jnp.float32)
    slot_index = jnp.sum(before * one_hot.astype(jnp.float32), axis=1).astype(jnp.int32)
    target = flat_expert * capacity + slot_index
    source_token = (
        jnp.zeros((experts_all * capacity,), jnp.int32)
        .at[target]
        .set(lax.iota(jnp.int32, assigned) // top_count)
    )
    filled = jnp.zeros((experts_all * capacity,), jnp.bool_).at[target].set(True)
    outgoing = jnp.where(filled[:, None], ffn_input[source_token], jnp.zeros((), jnp.bfloat16))
    arrived = lax.all_to_all(
        outgoing.reshape(experts_all, 1, capacity, model_width),
        ("sp", "dp"),
        split_axis=0,
        concat_axis=1,
        tiled=True,
    )
    served = expert_apply(arrived.reshape(-1, model_width), gate_w[0], up_w[0], down_w[0]).reshape(
        arrived.shape
    )
    returned = lax.all_to_all(served, ("sp", "dp"), split_axis=1, concat_axis=0, tiled=True)
    answers = returned.reshape(experts_all * capacity, model_width)[target].reshape(
        token_count, top_count, model_width
    )
    routed = jnp.sum(answers.astype(jnp.float32) * route_weight[0][:, :, None], axis=1)
    return (stream + routed).astype(jnp.bfloat16)[None]


def solution(mesh):
    return jax.shard_map(
        per_device,
        mesh=mesh,
        in_specs=(
            P("dp", "sp", None),
            P("dp", "sp", None),
            P("dp", "sp", None),
            P("dp", "sp", None),
            P("dp", "sp", None),
            P("dp", "sp", None),
            P(None, "sp"),
            P(None, "sp"),
            P(None, "sp"),
            P(None, "sp"),
            P(),
            P("dp", None),
            P(),
            P("dp", "sp", None),
            P("dp", "sp", None),
            P(("sp", "dp"), None, None),
            P(("sp", "dp"), None, None),
            P(("sp", "dp"), None, None),
        ),
        out_specs=P("dp", "sp", None),
        check_vma=False,
    )
```

profile of v0, /device:TPU:0, one launch (start us, length us, event | category | flops | bytes accessed | tf_op | source)
XLA Modules:
  0.0 593.2 jit_solution(14544832548649737198)
XLA Ops:
  9.2 7.3 %all-to-all-start.1 = ((bf16[8,2,512]{2,1,0:T(2,128)(2,1)}), bf16[8,2,512]{2,1,0:T(2,128)(2,1)S(1)}, u32[]{:S(2)}, u32[]{:S(2)}) async-start(bf16[8,2,512]{2,1,0:T(2,128)(2,1)} %reshape.329), calls=%async_computation.1 | async-start | bytes 32768 | tf_op jit(solution)/shard_map/all_to_all | solution.py:128
  22.7 2.4 copy.167
  25.2 11.5 %reduce.8 = bf16[2048,128]{1,0:T(8,128)(2,1)S(1)} reduce(bf16[2048,1,128]{2,1,0:T(2,128)(2,1)S(1)} %bitcast.256, bf16[]{:T(256)} %broadcast.189), dimensions={1}, to_apply=%bitcast.193.reduce_sub_computation | reduce | bytes 1048578
  38.4 11.5 %reduce.7 = bf16[2048,128]{1,0:T(8,128)(2,1)S(1)} reduce(bf16[2048,1,128]{2,1,0:T(2,128)(2,1)S(1)} %bitcast.257, bf16[]{:T(256)} %broadcast.189), dimensions={1}, to_apply=%bitcast.191.reduce_sub_computation | reduce | bytes 1048578
  51.6 11.8 %reduce.9 = bf16[2048,128]{1,0:T(8,128)(2,1)S(1)} reduce(bf16[2048,1,128]{2,1,0:T(2,128)(2,1)S(1)} %bitcast.258, bf16[]{:T(256)} %broadcast.189), dimensions={1}, to_apply=%bitcast.195.reduce_sub_computation | reduce | bytes 1048578
  64.4 6.0 %all-to-all-start = ((bf16[8,2,16384]{2,1,0:T(2,128)(2,1)}), bf16[8,2,16384]{2,1,0:T(2,128)(2,1)}, u32[]{:S(2)}, u32[]{:S(2)}) async-start(bf16[8,2,16384]{2,1,0:T(2,128)(2,1)} %reshape.333), calls=%async_computation | async-start | bytes 1048576 | tf_op jit(solution)/shard_map/all_to_all | solution.py:125
  71.8 47.4 %fusion.95 = f32[8,128,2,2]{3,0,1,2:T(8,128)S(1)} fusion(f32[8,128,2,2]{3,0,1,2:T(8,128)S(1)} %copy.202), kind=kOutput, calls=%fused_computation.155 | output fusion | flops 520192 | bytes 32768 | tf_op jit(solution)/shard_map/jit(cumsum)/reduce_window_sum | solution.py:36
  120.0 47.4 %fusion.94 = f32[8,128,2,2]{3,0,1,2:T(8,128)S(1)} fusion(f32[8,128,2,2]{3,0,1,2:T(8,128)S(1)} %copy.183), kind=kOutput, calls=%fused_computation.154 | output fusion | flops 520192 | bytes 32768 | tf_op jit(solution)/shard_map/jit(cumsum)/reduce_window_sum | solution.py:36
  170.5 6.0 %all-to-all-start.2 = ((bf16[8,2,16384]{2,1,0:T(2,128)(2,1)}), bf16[8,2,16384]{2,1,0:T(2,128)(2,1)}, u32[]{:S(2)}, u32[]{:S(2)}) async-start(bf16[8,2,16384]{2,1,0:T(2,128)(2,1)} %reshape.331), calls=%async_computation.2 | async-start | bytes 1048576 | tf_op jit(solution)/shard_map/all_to_all | solution.py:126
  183.8 2.2 reshape.334
  190.0 6.2 %all-to-all-start.3 = ((bf16[8,2,16384]{2,1,0:T(2,128)(2,1)}), bf16[8,2,16384]{2,1,0:T(2,128)(2,1)}, u32[]{:S(2)}, u32[]{:S(2)}) async-start(bf16[8,2,16384]{2,1,0:T(2,128)(2,1)} %reshape.335), calls=%async_computation.3 | async-start | bytes 1048576 | tf_op jit(solution)/shard_map/all_to_all | solution.py:127
  197.5 2.2 reshape.332
  200.3 2.7 copy_bitcast_fusion.1
  203.0 6.8 %rev.20 = f32[1024,2,128]{2,0,1:T(8,128)S(1)} reverse(f32[1024,2,128]{2,0,1:T(8,128)} %copy_bitcast_fusion.1), dimensions={0} | reverse | bytes 2097152 | tf_op jit(solution)/shard_map/jit(_flip)/rev | solution.py:75
  209.9 3.5 reshape.336
  215.7 2.6 copy.178
  218.3 6.2 %copy_bitcast_fusion = f32[1024,2,128]{2,0,1:T(8,128)} fusion(f32[256]{0:T(256)} %bitcast.284, f32[256]{0:T(256)} %bitcast.286, f32[256]{0:T(256)S(1)} %bitcast.276, f32[1024,256]{1,0:T(8,128)} %bitcast.240, f32[256]{0:T(256)S(1)} %bitcast.278, f32[256]{0:T(256)S(1)} %bitcast.280, f32[256]{0:T(256)} %bitcast.282, f32[256]{0:T(256)S(1)} %bitcast.274), kind=kLoop, calls=%fused_computation.43 | loop fusion | flops 4456448 | bytes 2104320 | tf_op jit(solution)/shard_map/reshape | solution.py:138
  224.5 6.8 %rev.21 = f32[1024,2,128]{2,0,1:T(8,128)S(1)} reverse(f32[1024,2,128]{2,0,1:T(8,128)} %copy_bitcast_fusion), dimensions={0} | reverse | bytes 2097152 | tf_op jit(solution)/shard_map/jit(_flip)/rev | solution.py:76
  231.3 3.3 convolution_bitcast_fusion.1
  234.7 2.6 copy.201
  238.5 2.3 fusion.43
  241.9 18.6 %while.27 = (s32[]{:T(128)}, f32[2,2,64,128]{3,2,1,0:T(8,128)S(1)}, f32[8,2,2,64,128]{4,3,2,1,0:T(8,128)}, f32[8,2,2]{2,1,0:T(2,128)}, f32[8,2,2,64,128]{4,3,2,1,0:T(8,128)}, /*index=5*/s32[]{:T(128)}, s32[]{:T(128)}) while((s32[]{:T(128)}, f32[2,2,64,128]{3,2,1,0:T(8,128)S(1)}, f32[8,2,2,64,128]{4,3,2,1,0:T(8,128)}, ...), condition=%wide.region_5.6_spmd.clone, body=%wide.region_4.5_spmd.clone.sunk | while | flops 131075 | bytes 656016 | solution.py:61
  260.6 3.5 fusion.33
  264.1 5.5 fusion.30
  271.5 5.6 rev.22
  283.9 3.3 convolution_bitcast_fusion.3
  287.2 2.6 copy.182
  291.0 2.3 fusion.46
  293.4 13.7 %while.26 = (s32[]{:T(128)}, f32[2,2,64,128]{3,2,1,0:T(8,128)S(1)}, f32[8,2,2,64,128]{4,3,2,1,0:T(8,128)S(1)}, f32[8,2,2]{2,1,0:T(2,128)}, f32[8,2,2,64,128]{4,3,2,1,0:T(8,128)}, /*index=5*/s32[]{:T(128)}, s32[]{:T(128)}) while((s32[]{:T(128)}, f32[2,2,64,128]{3,2,1,0:T(8,128)S(1)}, f32[8,2,2,64,128]{4,3,2,1,0:T(8,128)S(1)}, ...), condition=%wide.region_2.3_spmd.clone, body=%wide.region_1.2_spmd.clone.sunk | while | flops 131075 | bytes 655508 | solution.py:61
  307.0 2.3 fusion.34
  309.4 5.6 fusion.24
  316.8 3.8 reduce.10
  321.5 6.0 %all-to-all-start.4 = ((bf16[8,2,16384]{2,1,0:T(2,128)(2,1)}), bf16[8,2,16384]{2,1,0:T(2,128)(2,1)S(1)}, u32[]{:S(2)}, u32[]{:S(2)}) async-start(bf16[8,2,16384]{2,1,0:T(2,128)(2,1)} %reshape.337), calls=%async_computation.4 | async-start | bytes 1048576 | tf_op jit(solution)/shard_map/all_to_all | solution.py:146
  328.8 2.4 scatter_custom_fusion.1
  331.3 2.7 scatter_custom_fusion
  334.1 5.7 all-to-all-done.4
  344.0 4.8 multiply_reduce_fusion.1
  348.9 6.0 %gather_fusion = bf16[1024,2048]{1,0:T(8,128)(2,1)} fusion(bf16[128,2048]{1,0:T(8,128)(2,1)S(1)} %multiply_convert_fusion.1, s32[1024]{0:T(1024)S(1)} %fusion.78), kind=kCustom, calls=%fused_computation | custom fusion | bytes 8392704 | tf_op jit(solution)/shard_map/gather | solution.py:180
  354.9 2.5 broadcast_select_fusion
  357.5 97.6 %all_to_all.28 = bf16[32,1,32,2048]{3,2,1,0:T(8,128)(2,1)S(1)} all-to-all(bf16[32,1,32,2048]{3,2,1,0:T(8,128)(2,1)S(1)} %broadcast_select_fusion), channel_id=1, replica_groups=mesh['sp'=8,'dp'=4] {'sp','dp'}, dimensions={0} | all-to-all | bytes 8388608 | tf_op jit(solution)/shard_map/all_to_all | solution.py:181
  455.1 4.5 fusion.2
  459.7 5.7 multiply_convert_fusion
  465.3 6.1 %fusion.6 = bf16[1024,2048]{1,0:T(8,128)(2,1)} fusion(bf16[1024,1024]{1,0:T(8,128)(2,1)S(1)} %multiply_convert_fusion, bf16[1,1024,2048]{2,1,0:T(8,128)(2,1)S(1)} %copy-done.35), kind=kOutput, calls=%fused_computation.19 | convolution fusion | flops 4297064448 | bytes 10485760 | tf_op jit(solution)/shard_map/dot_general | solution.py:101
  471.5 4.0 all-to-all-start.6
  475.6 94.1 %all-to-all-done.6 = bf16[1,32,32,2048]{3,2,0,1:T(8,128)(2,1)} async-done(((bf16[1,32,32,2048]{3,2,0,1:T(8,128)(2,1)}), bf16[1,32,32,2048]{3,2,0,1:T(8,128)(2,1)}, u32[]{:S(2)}, u32[]{:S(2)}) %all-to-all-start.6) | async-done | bytes 4194336 | tf_op jit(solution)/shard_map/all_to_all | solution.py:191
  569.7 7.1 %gather_fusion.1 = bf16[512,2048]{1,0:T(8,128)(2,1)S(1)} fusion(bf16[1024,2048]{1,0:T(8,128)(2,1)} %bitcast.69, s32[1024]{0:T(1024)S(1)} %pad_clamp_fusion), kind=kCustom, calls=%fused_computation.1 | custom fusion | bytes 4196352 | tf_op jit(solution)/shard_map/gather | solution.py:192
  576.8 3.0 reshape.273
  579.8 5.4 multiply_reduce_fusion
  (230 shorter events, 86.9 us)
Async XLA Ops:
  6.5 31.1 %copy-start.7 = (bf16[1,128,2048]{2,1,0:T(8,128)(2,1)S(1)}, bf16[1,128,2048]{2,1,0:T(8,128)(2,1)}, u32[]{:S(2)}) copy-start(bf16[1,128,2048]{2,1,0:T(8,128)(2,1)} %param.24) | copy-start | bytes 1572868
  9.2 55.2 %all-to-all-start.1 = ((bf16[8,2,512]{2,1,0:T(2,128)(2,1)}), bf16[8,2,512]{2,1,0:T(2,128)(2,1)S(1)}, u32[]{:S(2)}, u32[]{:S(2)}) async-start(bf16[8,2,512]{2,1,0:T(2,128)(2,1)} %reshape.329), calls=%async_computation.1 | async-start | bytes 32768 | tf_op jit(solution)/shard_map/all_to_all | solution.py:128
  16.5 327.5 %all-gather.2.cloned.1.call-start = ((), (), s32[]{:S(2)}) async-start(), calls=%async_computation.7 | async-start | bytes 10485760 | tf_op jit(solution)/shard_map/all_gather | solution.py:153
  22.7 28.1 %copy-start.8 = (bf16[1,128,2048]{2,1,0:T(8,128)(2,1)S(1)}, bf16[1,128,2048]{2,1,0:T(8,128)(2,1)}, u32[]{:S(2)}) copy-start(bf16[1,128,2048]{2,1,0:T(8,128)(2,1)} %param.25) | copy-start | bytes 1572868
  64.4 106.2 %all-to-all-start = ((bf16[8,2,16384]{2,1,0:T(2,128)(2,1)}), bf16[8,2,16384]{2,1,0:T(2,128)(2,1)}, u32[]{:S(2)}, u32[]{:S(2)}) async-start(bf16[8,2,16384]{2,1,0:T(2,128)(2,1)} %reshape.333), calls=%async_computation | async-start | bytes 1048576 | tf_op jit(solution)/shard_map/all_to_all | solution.py:125
  170.5 19.5 %all-to-all-start.2 = ((bf16[8,2,16384]{2,1,0:T(2,128)(2,1)}), bf16[8,2,16384]{2,1,0:T(2,128)(2,1)}, u32[]{:S(2)}, u32[]{:S(2)}) async-start(bf16[8,2,16384]{2,1,0:T(2,128)(2,1)} %reshape.331), calls=%async_computation.2 | async-start | bytes 1048576 | tf_op jit(solution)/shard_map/all_to_all | solution.py:126
  190.0 19.9 %all-to-all-start.3 = ((bf16[8,2,16384]{2,1,0:T(2,128)(2,1)}), bf16[8,2,16384]{2,1,0:T(2,128)(2,1)}, u32[]{:S(2)}, u32[]{:S(2)}) async-start(bf16[8,2,16384]{2,1,0:T(2,128)(2,1)} %reshape.335), calls=%async_computation.3 | async-start | bytes 1048576 | tf_op jit(solution)/shard_map/all_to_all | solution.py:127
  196.3 3.9 copy-start.18
  196.3 3.9 copy-start.20
  196.3 3.9 copy-start.22
  196.3 3.9 copy-start.24
  200.2 15.5 %copy-start = (f32[1,8,128,256]{3,2,1,0:T(8,128)}, f32[1,8,128,256]{3,2,1,0:T(8,128)S(1)}, u32[]{:S(2)}) copy-start(f32[1,8,128,256]{3,2,1,0:T(8,128)S(1)} %copy.175) | copy-start | bytes 3145732
  203.0 15.3 %copy-start.10 = (f32[1,256]{1,0:T(1,128)S(1)}, f32[1,256]{1,0:T(1,128)}, u32[]{:S(2)}) copy-start(f32[1,256]{1,0:T(1,128)} %get-tuple-element.177) | copy-start | bytes 3076
  203.0 15.3 %copy-start.11 = (f32[1,256]{1,0:T(1,128)S(1)}, f32[1,256]{1,0:T(1,128)}, u32[]{:S(2)}) copy-start(f32[1,256]{1,0:T(1,128)} %get-tuple-element.178) | copy-start | bytes 3076
  203.0 15.3 %copy-start.12 = (f32[1,256]{1,0:T(1,128)S(1)}, f32[1,256]{1,0:T(1,128)}, u32[]{:S(2)}) copy-start(f32[1,256]{1,0:T(1,128)} %get-tuple-element.179) | copy-start | bytes 3076
  203.0 15.3 %copy-start.13 = (f32[1,256]{1,0:T(1,128)S(1)}, f32[1,256]{1,0:T(1,128)}, u32[]{:S(2)}) copy-start(f32[1,256]{1,0:T(1,128)} %get-tuple-element.180) | copy-start | bytes 3076
  240.8 23.3 %copy-start.3 = (f32[32,8,8,128]{3,2,1,0:T(8,128)S(1)}, f32[32,8,8,128]{3,2,1,0:T(8,128)}, u32[]{:S(2)}) copy-start(f32[32,8,8,128]{3,2,1,0:T(8,128)} %copy.245) | copy-start | bytes 3145732
  269.6 8.7 %copy-start.1 = (f32[1,8,128,256]{3,2,1,0:T(8,128)S(1)}, f32[1,8,128,256]{3,2,1,0:T(8,128)}, u32[]{:S(2)}) copy-start(f32[1,8,128,256]{3,2,1,0:T(8,128)} %copy-done) | copy-start | bytes 3145732
  269.6 8.7 %copy-start.19 = (f32[1,256]{1,0:T(1,128)S(1)}, f32[1,256]{1,0:T(1,128)}, u32[]{:S(2)}) copy-start(f32[1,256]{1,0:T(1,128)} %get-tuple-element.191) | copy-start | bytes 3076
  269.6 8.7 %copy-start.21 = (f32[1,256]{1,0:T(1,128)S(1)}, f32[1,256]{1,0:T(1,128)}, u32[]{:S(2)}) copy-start(f32[1,256]{1,0:T(1,128)} %get-tuple-element.192) | copy-start | bytes 3076
  269.6 8.7 %copy-start.23 = (f32[1,256]{1,0:T(1,128)S(1)}, f32[1,256]{1,0:T(1,128)}, u32[]{:S(2)}) copy-start(f32[1,256]{1,0:T(1,128)} %get-tuple-element.193) | copy-start | bytes 3076
  269.6 8.7 %copy-start.25 = (f32[1,256]{1,0:T(1,128)S(1)}, f32[1,256]{1,0:T(1,128)}, u32[]{:S(2)}) copy-start(f32[1,256]{1,0:T(1,128)} %get-tuple-element.194) | copy-start | bytes 3076
  269.6 8.7 %copy-start.26 = (f32[1,256]{1,0:T(1,128)S(1)}, f32[1,256]{1,0:T(1,128)}, u32[]{:S(2)}) copy-start(f32[1,256]{1,0:T(1,128)} %get-tuple-element.195) | copy-start | bytes 3076
  269.7 8.7 %copy-start.27 = (f32[1,256]{1,0:T(1,128)S(1)}, f32[1,256]{1,0:T(1,128)}, u32[]{:S(2)}) copy-start(f32[1,256]{1,0:T(1,128)} %get-tuple-element.196) | copy-start | bytes 3076
  269.7 8.7 %copy-start.28 = (f32[1,256]{1,0:T(1,128)S(1)}, f32[1,256]{1,0:T(1,128)}, u32[]{:S(2)}) copy-start(f32[1,256]{1,0:T(1,128)} %get-tuple-element.197) | copy-start | bytes 3076
  271.5 8.5 %copy-start.2 = (f32[1,8,128,256]{3,2,1,0:T(8,128)S(1)}, f32[1,8,128,256]{3,2,1,0:T(8,128)}, u32[]{:S(2)}) copy-start(f32[1,8,128,256]{3,2,1,0:T(8,128)} %copy.178) | copy-start | bytes 3145732
  271.5 8.5 %copy-start.14 = (f32[1,256]{1,0:T(1,128)S(1)}, f32[1,256]{1,0:T(1,128)}, u32[]{:S(2)}) copy-start(f32[1,256]{1,0:T(1,128)} %get-tuple-element.180) | copy-start | bytes 3076
  271.5 8.5 %copy-start.15 = (f32[1,256]{1,0:T(1,128)S(1)}, f32[1,256]{1,0:T(1,128)}, u32[]{:S(2)}) copy-start(f32[1,256]{1,0:T(1,128)} %get-tuple-element.181) | copy-start | bytes 3076
  271.5 8.5 %copy-start.16 = (f32[1,256]{1,0:T(1,128)S(1)}, f32[1,256]{1,0:T(1,128)}, u32[]{:S(2)}) copy-start(f32[1,256]{1,0:T(1,128)} %get-tuple-element.182) | copy-start | bytes 3076
  271.5 8.5 %copy-start.17 = (f32[1,256]{1,0:T(1,128)S(1)}, f32[1,256]{1,0:T(1,128)}, u32[]{:S(2)}) copy-start(f32[1,256]{1,0:T(1,128)} %get-tuple-element.183) | copy-start | bytes 3076
  282.1 7.8 %copy-start.4 = (f32[32,8,8,128]{3,2,1,0:T(8,128)S(1)}, f32[32,8,8,128]{3,2,1,0:T(8,128)}, u32[]{:S(2)}) copy-start(f32[32,8,8,128]{3,2,1,0:T(8,128)} %copy.244) | copy-start | bytes 3145732
  293.3 16.1 %copy-start.6 = (f32[8,128,2,2,64]{1,0,4,3,2:T(8,128)S(1)}, f32[8,128,2,2,64]{1,0,4,3,2:T(8,128)}, u32[]{:S(2)}) copy-start(f32[8,128,2,2,64]{1,0,4,3,2:T(8,128)} %get-tuple-element.170) | copy-start | bytes 3145732
  309.4 6.4 %copy-start.5 = (f32[1024,4,64]{0,2,1:T(8,128)S(1)}, f32[1024,4,64]{0,2,1:T(8,128)}, u32[]{:S(2)}) copy-start(f32[1024,4,64]{0,2,1:T(8,128)} %rev.22) | copy-start | bytes 3145732
  315.9 11.6 %copy-start.9 = (bf16[1,128,2048]{2,1,0:T(8,128)(2,1)S(1)}, bf16[1,128,2048]{2,1,0:T(8,128)(2,1)}, u32[]{:S(2)}) copy-start(bf16[1,128,2048]{2,1,0:T(8,128)(2,1)} %param.27) | copy-start | bytes 1572868
  315.9 12.1 %copy-start.31 = (s32[1,128,4]{1,2,0:T(4,128)S(1)}, s32[1,128,4]{1,2,0:T(4,128)}, u32[]{:S(2)}) copy-start(s32[1,128,4]{1,2,0:T(4,128)} %param.35) | copy-start | bytes 6148
  321.5 18.2 %all-to-all-start.4 = ((bf16[8,2,16384]{2,1,0:T(2,128)(2,1)}), bf16[8,2,16384]{2,1,0:T(2,128)(2,1)S(1)}, u32[]{:S(2)}, u32[]{:S(2)}) async-start(bf16[8,2,16384]{2,1,0:T(2,128)(2,1)} %reshape.337), calls=%async_computation.4 | async-start | bytes 1048576 | tf_op jit(solution)/shard_map/all_to_all | solution.py:146
  328.3 15.3 %copy-start.29 = (f32[2048]{0:T(1024)S(1)}, f32[2048]{0:T(1024)}, u32[]{:S(2)}) copy-start(f32[2048]{0:T(1024)} %param.32) | copy-start | bytes 24580
  343.9 4.8 copy-start.30
  357.5 97.6 %copy-start.33 = (bf16[1,2048,1024]{2,1,0:T(8,128)(2,1)S(1)}, bf16[1,2048,1024]{2,1,0:T(8,128)(2,1)}, u32[]{:S(2)}) copy-start(bf16[1,2048,1024]{2,1,0:T(8,128)(2,1)} %param.37) | copy-start | bytes 12582916
  455.1 4.5 copy-start.34
  459.6 5.7 copy-start.35
  471.5 4.0 copy-start.32
  471.5 98.2 %all-to-all-start.6 = ((bf16[1,32,32,2048]{3,2,0,1:T(8,128)(2,1)}), bf16[1,32,32,2048]{3,2,0,1:T(8,128)(2,1)}, u32[]{:S(2)}, u32[]{:S(2)}) async-start(bf16[1,32,32,2048]{3,2,0,1:T(8,128)(2,1)} %bitcast.249), calls=%async_computation.6 | async-start | bytes 8388608 | tf_op jit(solution)/shard_map/all_to_all | solution.py:191
Sparse Core Ops, SparseCore 0:
  18.9 59.6 all-gather.1
where the time goes:
time: 604 us; the launch traced here: 593 us
  other arithmetic  188 us (31%)
  local copies, waits for them, and re-layouts  107 us (18%)
  waiting for transfers between devices  101 us (17%)
  blocking collectives  97.6 us (16%)
  matrix products  49.4 us (8%)
  starting transfers between devices  35.4 us (6%)
  between operations  14.5 us (2%)
    all_to_all x1, blocking collectives, per_device(): lax.all_to_all(outgoing.reshape(experts_all, 1, capacity, model_width), (...  97.6 us
    another operation x2, other arithmetic, ssd_direction(): jnp.cumsum((-step_size * rates).reshape(blocks, BLOCK, group_count, per_g...  94.9 us
    all_to_all x1, waiting for transfers between devices, per_device(): lax.all_to_all(served, ('sp', 'dp'), split_axis=1, concat_axis=0, tiled=T...  94.1 us
    unnamed x8, other arithmetic  39.5 us
    unnamed x95, local copies, waits for them, and re-layouts  22.3 us
    add x16, other arithmetic, advance(): return (factor[..., None, None] * running + block_state, running)  15.7 us
  transfers between devices with their start and end apart: 7, of which 3 were waited for; matrix products, arithmetic and copies ran while one was open for 50% of the time, Pallas kernels for 0%

commit v1 on v0

--- a/solution.py
+++ b/solution.py
@@ -188,7 +188,12 @@
     served = expert_apply(arrived.reshape(-1, model_width), gate_w[0], up_w[0], down_w[0]).reshape(
         arrived.shape
     )
-    returned = lax.all_to_all(served, ("sp", "dp"), split_axis=1, concat_axis=0, tiled=True)
+    returned = jnp.concatenate(
+        lax.all_to_all(
+            jnp.stack(jnp.split(served, lax.axis_size(("sp", "dp")), axis=1)), ("sp", "dp"), 0, 0
+        ),
+        axis=0,
+    )
     answers = returned.reshape(experts_all * capacity, model_width)[target].reshape(
         token_count, top_count, model_width
     )

time: 604 us -> 624 us (1.033)
  local copies, waits for them, and re-layouts: 107 us -> 128 us
    unnamed x95 -> x126, local copies, waits for them, and re-layouts: 22.3 us -> 42.9 us
  transfers between devices with their start and end apart: 7 -> 7, of which waited for: 3 -> 3; matrix products, arithmetic and copies ran while one was open for 50% -> 48% of each run, Pallas kernels for 0% -> 0%
where the time goes in v1:
time: 624 us; the launch traced here: 613 us
  other arithmetic  187 us (30%)
  local copies, waits for them, and re-layouts  128 us (21%)
  waiting for transfers between devices  101 us (16%)
  blocking collectives  97.4 us (16%)
  matrix products  48 us (8%)
  starting transfers between devices  35.3 us (6%)
  between operations  14.9 us (2%)
    all_to_all x1, blocking collectives, per_device(): lax.all_to_all(outgoing.reshape(experts_all, 1, capacity, model_width), (...  97.4 us
    another operation x2, other arithmetic, ssd_direction(): jnp.cumsum((-step_size * rates).reshape(blocks, BLOCK, group_count, per_g...  94.9 us
    all_to_all x1, waiting for transfers between devices, per_device(): lax.all_to_all(jnp.stack(jnp.split(served, lax.axis_size(('sp', 'dp')), a...  94.1 us
    unnamed x126, local copies, waits for them, and re-layouts  42.9 us
    unnamed x8, other arithmetic  39.3 us
    add x16, other arithmetic, advance(): return (factor[..., None, None] * running + block_state, running)  15.7 us
  transfers between devices with their start and end apart: 7, of which 3 were waited for; matrix products, arithmetic and copies ran while one was open for 48% of the time, Pallas kernels for 0%

profile of v1, /device:TPU:0, one launch (start us, length us, event | category | flops | bytes accessed | tf_op | source)
XLA Modules:
  0.0 613.1 jit_solution(1986890154848243864)
XLA Ops:
  9.2 7.3 %all-to-all-start.1 = ((bf16[8,2,512]{2,1,0:T(2,128)(2,1)}), bf16[8,2,512]{2,1,0:T(2,128)(2,1)S(1)}, u32[]{:S(2)}, u32[]{:S(2)}) async-start(bf16[8,2,512]{2,1,0:T(2,128)(2,1)} %reshape.321), calls=%async_computation.1 | async-start | bytes 32768 | tf_op jit(solution)/shard_map/all_to_all | solution.py:128
  22.7 2.4 copy.167
  25.2 11.5 %reduce.8 = bf16[2048,128]{1,0:T(8,128)(2,1)S(1)} reduce(bf16[2048,1,128]{2,1,0:T(2,128)(2,1)S(1)} %bitcast.413, bf16[]{:T(256)} %broadcast.189), dimensions={1}, to_apply=%bitcast.319.reduce_sub_computation | reduce | bytes 1048578
  38.4 11.5 %reduce.7 = bf16[2048,128]{1,0:T(8,128)(2,1)S(1)} reduce(bf16[2048,1,128]{2,1,0:T(2,128)(2,1)S(1)} %bitcast.414, bf16[]{:T(256)} %broadcast.189), dimensions={1}, to_apply=%bitcast.317.reduce_sub_computation | reduce | bytes 1048578
  51.6 11.7 %reduce.9 = bf16[2048,128]{1,0:T(8,128)(2,1)S(1)} reduce(bf16[2048,1,128]{2,1,0:T(2,128)(2,1)S(1)} %bitcast.415, bf16[]{:T(256)} %broadcast.189), dimensions={1}, to_apply=%bitcast.321.reduce_sub_computation | reduce | bytes 1048578
  64.3 6.0 all-to-all-start
  71.7 47.4 %fusion.127 = f32[8,128,2,2]{3,0,1,2:T(8,128)S(1)} fusion(f32[8,128,2,2]{3,0,1,2:T(8,128)S(1)} %copy.202), kind=kOutput, calls=%fused_computation.219 | output fusion | flops 520192 | bytes 32768 | tf_op jit(solution)/shard_map/jit(cumsum)/reduce_window_sum | solution.py:36
  119.8 47.4 %fusion.126 = f32[8,128,2,2]{3,0,1,2:T(8,128)S(1)} fusion(f32[8,128,2,2]{3,0,1,2:T(8,128)S(1)} %copy.183), kind=kOutput, calls=%fused_computation.218 | output fusion | flops 520192 | bytes 32768 | tf_op jit(solution)/shard_map/jit(cumsum)/reduce_window_sum | solution.py:36
  170.4 6.0 all-to-all-start.2
  183.7 2.2 reshape.326
  189.9 5.9 all-to-all-start.3
  197.1 2.2 reshape.324
  199.9 2.7 copy_bitcast_fusion.1
  202.6 6.8 %rev.20 = f32[1024,2,128]{2,0,1:T(8,128)S(1)} reverse(f32[1024,2,128]{2,0,1:T(8,128)} %copy_bitcast_fusion.1), dimensions={0} | reverse | bytes 2097152 | tf_op jit(solution)/shard_map/jit(_flip)/rev | solution.py:75
  209.4 3.5 reshape.328
  215.3 2.6 copy.178
  217.9 6.2 %copy_bitcast_fusion = f32[1024,2,128]{2,0,1:T(8,128)} fusion(f32[256]{0:T(256)} %bitcast.441, f32[256]{0:T(256)} %bitcast.443, f32[256]{0:T(256)S(1)} %bitcast.433, f32[1024,256]{1,0:T(8,128)} %bitcast.366, f32[256]{0:T(256)S(1)} %bitcast.435, f32[256]{0:T(256)S(1)} %bitcast.437, f32[256]{0:T(256)} %bitcast.439, f32[256]{0:T(256)S(1)} %bitcast.431), kind=kLoop, calls=%fused_computation.43 | loop fusion | flops 4456448 | bytes 2104320 | tf_op jit(solution)/shard_map/reshape | solution.py:138
  224.1 6.8 %rev.21 = f32[1024,2,128]{2,0,1:T(8,128)S(1)} reverse(f32[1024,2,128]{2,0,1:T(8,128)} %copy_bitcast_fusion), dimensions={0} | reverse | bytes 2097152 | tf_op jit(solution)/shard_map/jit(_flip)/rev | solution.py:76
  230.9 3.3 convolution_bitcast_fusion.1
  234.2 2.6 copy.201
  238.1 2.3 fusion.43
  241.5 18.9 %while.27 = (s32[]{:T(128)}, f32[2,2,64,128]{3,2,1,0:T(8,128)S(1)}, f32[8,2,2,64,128]{4,3,2,1,0:T(8,128)}, f32[8,2,2]{2,1,0:T(2,128)}, f32[8,2,2,64,128]{4,3,2,1,0:T(8,128)}, /*index=5*/s32[]{:T(128)}, s32[]{:T(128)}) while((s32[]{:T(128)}, f32[2,2,64,128]{3,2,1,0:T(8,128)S(1)}, f32[8,2,2,64,128]{4,3,2,1,0:T(8,128)}, ...), condition=%wide.region_5.6_spmd.clone, body=%wide.region_4.5_spmd.clone.sunk | while | flops 131075 | bytes 656016 | solution.py:61
  260.4 3.5 fusion.33
  263.9 5.5 fusion.30
  271.3 5.6 rev.22
  283.7 3.3 convolution_bitcast_fusion.3
  287.0 2.6 copy.182
  290.8 2.3 fusion.46
  293.2 13.6 %while.26 = (s32[]{:T(128)}, f32[2,2,64,128]{3,2,1,0:T(8,128)S(1)}, f32[8,2,2,64,128]{4,3,2,1,0:T(8,128)S(1)}, f32[8,2,2]{2,1,0:T(2,128)}, f32[8,2,2,64,128]{4,3,2,1,0:T(8,128)}, /*index=5*/s32[]{:T(128)}, s32[]{:T(128)}) while((s32[]{:T(128)}, f32[2,2,64,128]{3,2,1,0:T(8,128)S(1)}, f32[8,2,2,64,128]{4,3,2,1,0:T(8,128)S(1)}, ...), condition=%wide.region_2.3_spmd.clone, body=%wide.region_1.2_spmd.clone.sunk | while | flops 131075 | bytes 655508 | solution.py:61
  306.8 2.3 fusion.34
  309.1 5.6 fusion.24
  316.6 3.8 reduce.10
  321.3 6.0 all-to-all-start.4
  328.6 2.4 scatter_custom_fusion.1
  331.0 2.7 scatter_custom_fusion
  333.8 5.7 all-to-all-done.4
  343.7 4.8 multiply_reduce_fusion.1
  348.7 6.0 gather_fusion
  354.7 2.5 broadcast_select_fusion
  357.3 97.4 %all_to_all.28 = bf16[32,1,32,2048]{3,2,1,0:T(8,128)(2,1)S(1)} all-to-all(bf16[32,1,32,2048]{3,2,1,0:T(8,128)(2,1)S(1)} %broadcast_select_fusion), channel_id=1, replica_groups=mesh['sp'=8,'dp'=4] {'sp','dp'}, dimensions={0} | all-to-all | bytes 8388608 | tf_op jit(solution)/shard_map/all_to_all | solution.py:181
  454.6 4.5 fusion.2
  459.2 5.7 multiply_convert_fusion
  464.9 4.8 fusion.6
  491.0 4.1 all-to-all-start.6
  495.2 94.1 %all-to-all-done.6 = bf16[32,1,1,32,2048]{4,3,2,1,0:T(8,128)(2,1)} async-done(((bf16[32,1,1,32,2048]{4,3,2,1,0:T(8,128)(2,1)}), bf16[32,1,1,32,2048]{4,3,2,1,0:T(8,128)(2,1)}, u32[]{:S(2)}, u32[]{:S(2)}) %all-to-all-start.6) | async-done | bytes 4194336 | tf_op jit(solution)/shard_map/all_to_all | solution.py:192
  589.3 7.1 %gather_fusion.1 = bf16[512,2048]{1,0:T(8,128)(2,1)S(1)} fusion(bf16[1024,2048]{1,0:T(8,128)(2,1)} %bitcast.100, s32[1024]{0:T(1024)S(1)} %pad_clamp_fusion), kind=kCustom, calls=%fused_computation.1 | custom fusion | bytes 4196352 | tf_op jit(solution)/shard_map/gather | solution.py:197
  596.4 3.0 reshape.265
  599.4 5.4 multiply_reduce_fusion
  (262 shorter events, 108.2 us)
Async XLA Ops:
  6.5 31.1 %copy-start.7 = (bf16[1,128,2048]{2,1,0:T(8,128)(2,1)S(1)}, bf16[1,128,2048]{2,1,0:T(8,128)(2,1)}, u32[]{:S(2)}) copy-start(bf16[1,128,2048]{2,1,0:T(8,128)(2,1)} %param.24) | copy-start | bytes 1572868
  9.2 55.0 %all-to-all-start.1 = ((bf16[8,2,512]{2,1,0:T(2,128)(2,1)}), bf16[8,2,512]{2,1,0:T(2,128)(2,1)S(1)}, u32[]{:S(2)}, u32[]{:S(2)}) async-start(bf16[8,2,512]{2,1,0:T(2,128)(2,1)} %reshape.321), calls=%async_computation.1 | async-start | bytes 32768 | tf_op jit(solution)/shard_map/all_to_all | solution.py:128
  16.5 327.2 %all-gather.2.cloned.1.call-start = ((), (), s32[]{:S(2)}) async-start(), calls=%async_computation.7 | async-start | bytes 10485760 | tf_op jit(solution)/shard_map/all_gather | solution.py:153
  22.7 28.1 %copy-start.8 = (bf16[1,128,2048]{2,1,0:T(8,128)(2,1)S(1)}, bf16[1,128,2048]{2,1,0:T(8,128)(2,1)}, u32[]{:S(2)}) copy-start(bf16[1,128,2048]{2,1,0:T(8,128)(2,1)} %param.25) | copy-start | bytes 1572868
  64.3 106.2 %all-to-all-start = ((bf16[8,2,16384]{2,1,0:T(2,128)(2,1)}), bf16[8,2,16384]{2,1,0:T(2,128)(2,1)}, u32[]{:S(2)}, u32[]{:S(2)}) async-start(bf16[8,2,16384]{2,1,0:T(2,128)(2,1)} %reshape.325), calls=%async_computation | async-start | bytes 1048576 | tf_op jit(solution)/shard_map/all_to_all | solution.py:125
  170.4 19.5 %all-to-all-start.2 = ((bf16[8,2,16384]{2,1,0:T(2,128)(2,1)}), bf16[8,2,16384]{2,1,0:T(2,128)(2,1)}, u32[]{:S(2)}, u32[]{:S(2)}) async-start(bf16[8,2,16384]{2,1,0:T(2,128)(2,1)} %reshape.323), calls=%async_computation.2 | async-start | bytes 1048576 | tf_op jit(solution)/shard_map/all_to_all | solution.py:126
  189.9 19.6 %all-to-all-start.3 = ((bf16[8,2,16384]{2,1,0:T(2,128)(2,1)}), bf16[8,2,16384]{2,1,0:T(2,128)(2,1)}, u32[]{:S(2)}, u32[]{:S(2)}) async-start(bf16[8,2,16384]{2,1,0:T(2,128)(2,1)} %reshape.327), calls=%async_computation.3 | async-start | bytes 1048576 | tf_op jit(solution)/shard_map/all_to_all | solution.py:127
  195.9 3.9 copy-start.18
  195.9 3.9 copy-start.20
  195.9 3.9 copy-start.22
  195.9 3.9 copy-start.24
  199.8 15.5 %copy-start = (f32[1,8,128,256]{3,2,1,0:T(8,128)}, f32[1,8,128,256]{3,2,1,0:T(8,128)S(1)}, u32[]{:S(2)}) copy-start(f32[1,8,128,256]{3,2,1,0:T(8,128)S(1)} %copy.175) | copy-start | bytes 3145732
  202.6 15.3 %copy-start.10 = (f32[1,256]{1,0:T(1,128)S(1)}, f32[1,256]{1,0:T(1,128)}, u32[]{:S(2)}) copy-start(f32[1,256]{1,0:T(1,128)} %get-tuple-element.177) | copy-start | bytes 3076
  202.6 15.3 %copy-start.11 = (f32[1,256]{1,0:T(1,128)S(1)}, f32[1,256]{1,0:T(1,128)}, u32[]{:S(2)}) copy-start(f32[1,256]{1,0:T(1,128)} %get-tuple-element.178) | copy-start | bytes 3076
  202.6 15.3 %copy-start.12 = (f32[1,256]{1,0:T(1,128)S(1)}, f32[1,256]{1,0:T(1,128)}, u32[]{:S(2)}) copy-start(f32[1,256]{1,0:T(1,128)} %get-tuple-element.179) | copy-start | bytes 3076
  202.6 15.3 %copy-start.13 = (f32[1,256]{1,0:T(1,128)S(1)}, f32[1,256]{1,0:T(1,128)}, u32[]{:S(2)}) copy-start(f32[1,256]{1,0:T(1,128)} %get-tuple-element.180) | copy-start | bytes 3076
  240.4 23.5 %copy-start.3 = (f32[32,8,8,128]{3,2,1,0:T(8,128)S(1)}, f32[32,8,8,128]{3,2,1,0:T(8,128)}, u32[]{:S(2)}) copy-start(f32[32,8,8,128]{3,2,1,0:T(8,128)} %copy.244) | copy-start | bytes 3145732
  269.4 8.7 %copy-start.1 = (f32[1,8,128,256]{3,2,1,0:T(8,128)S(1)}, f32[1,8,128,256]{3,2,1,0:T(8,128)}, u32[]{:S(2)}) copy-start(f32[1,8,128,256]{3,2,1,0:T(8,128)} %copy-done) | copy-start | bytes 3145732
  269.4 8.7 %copy-start.19 = (f32[1,256]{1,0:T(1,128)S(1)}, f32[1,256]{1,0:T(1,128)}, u32[]{:S(2)}) copy-start(f32[1,256]{1,0:T(1,128)} %get-tuple-element.191) | copy-start | bytes 3076
  269.4 8.7 %copy-start.21 = (f32[1,256]{1,0:T(1,128)S(1)}, f32[1,256]{1,0:T(1,128)}, u32[]{:S(2)}) copy-start(f32[1,256]{1,0:T(1,128)} %get-tuple-element.192) | copy-start | bytes 3076
  269.4 8.7 %copy-start.23 = (f32[1,256]{1,0:T(1,128)S(1)}, f32[1,256]{1,0:T(1,128)}, u32[]{:S(2)}) copy-start(f32[1,256]{1,0:T(1,128)} %get-tuple-element.193) | copy-start | bytes 3076
  269.4 8.7 %copy-start.25 = (f32[1,256]{1,0:T(1,128)S(1)}, f32[1,256]{1,0:T(1,128)}, u32[]{:S(2)}) copy-start(f32[1,256]{1,0:T(1,128)} %get-tuple-element.194) | copy-start | bytes 3076
  269.4 8.7 %copy-start.26 = (f32[1,256]{1,0:T(1,128)S(1)}, f32[1,256]{1,0:T(1,128)}, u32[]{:S(2)}) copy-start(f32[1,256]{1,0:T(1,128)} %get-tuple-element.195) | copy-start | bytes 3076
  269.4 8.7 %copy-start.27 = (f32[1,256]{1,0:T(1,128)S(1)}, f32[1,256]{1,0:T(1,128)}, u32[]{:S(2)}) copy-start(f32[1,256]{1,0:T(1,128)} %get-tuple-element.196) | copy-start | bytes 3076
  269.5 8.7 %copy-start.28 = (f32[1,256]{1,0:T(1,128)S(1)}, f32[1,256]{1,0:T(1,128)}, u32[]{:S(2)}) copy-start(f32[1,256]{1,0:T(1,128)} %get-tuple-element.197) | copy-start | bytes 3076
  271.3 8.5 %copy-start.2 = (f32[1,8,128,256]{3,2,1,0:T(8,128)S(1)}, f32[1,8,128,256]{3,2,1,0:T(8,128)}, u32[]{:S(2)}) copy-start(f32[1,8,128,256]{3,2,1,0:T(8,128)} %copy.178) | copy-start | bytes 3145732
  271.3 8.5 %copy-start.14 = (f32[1,256]{1,0:T(1,128)S(1)}, f32[1,256]{1,0:T(1,128)}, u32[]{:S(2)}) copy-start(f32[1,256]{1,0:T(1,128)} %get-tuple-element.180) | copy-start | bytes 3076
  271.3 8.5 %copy-start.15 = (f32[1,256]{1,0:T(1,128)S(1)}, f32[1,256]{1,0:T(1,128)}, u32[]{:S(2)}) copy-start(f32[1,256]{1,0:T(1,128)} %get-tuple-element.181) | copy-start | bytes 3076
  271.3 8.5 %copy-start.16 = (f32[1,256]{1,0:T(1,128)S(1)}, f32[1,256]{1,0:T(1,128)}, u32[]{:S(2)}) copy-start(f32[1,256]{1,0:T(1,128)} %get-tuple-element.182) | copy-start | bytes 3076
  271.3 8.5 %copy-start.17 = (f32[1,256]{1,0:T(1,128)S(1)}, f32[1,256]{1,0:T(1,128)}, u32[]{:S(2)}) copy-start(f32[1,256]{1,0:T(1,128)} %get-tuple-element.183) | copy-start | bytes 3076
  281.9 7.8 %copy-start.4 = (f32[32,8,8,128]{3,2,1,0:T(8,128)S(1)}, f32[32,8,8,128]{3,2,1,0:T(8,128)}, u32[]{:S(2)}) copy-start(f32[32,8,8,128]{3,2,1,0:T(8,128)} %copy.243) | copy-start | bytes 3145732
  293.0 16.1 %copy-start.6 = (f32[8,128,2,2,64]{1,0,4,3,2:T(8,128)S(1)}, f32[8,128,2,2,64]{1,0,4,3,2:T(8,128)}, u32[]{:S(2)}) copy-start(f32[8,128,2,2,64]{1,0,4,3,2:T(8,128)} %get-tuple-element.170) | copy-start | bytes 3145732
  309.1 6.4 %copy-start.5 = (f32[1024,4,64]{0,2,1:T(8,128)S(1)}, f32[1024,4,64]{0,2,1:T(8,128)}, u32[]{:S(2)}) copy-start(f32[1024,4,64]{0,2,1:T(8,128)} %rev.22) | copy-start | bytes 3145732
  315.7 11.6 %copy-start.9 = (bf16[1,128,2048]{2,1,0:T(8,128)(2,1)S(1)}, bf16[1,128,2048]{2,1,0:T(8,128)(2,1)}, u32[]{:S(2)}) copy-start(bf16[1,128,2048]{2,1,0:T(8,128)(2,1)} %param.27) | copy-start | bytes 1572868
  315.7 12.1 %copy-start.31 = (s32[1,128,4]{1,2,0:T(4,128)S(1)}, s32[1,128,4]{1,2,0:T(4,128)}, u32[]{:S(2)}) copy-start(s32[1,128,4]{1,2,0:T(4,128)} %param.35) | copy-start | bytes 6148
  321.3 18.2 %all-to-all-start.4 = ((bf16[8,2,16384]{2,1,0:T(2,128)(2,1)}), bf16[8,2,16384]{2,1,0:T(2,128)(2,1)S(1)}, u32[]{:S(2)}, u32[]{:S(2)}) async-start(bf16[8,2,16384]{2,1,0:T(2,128)(2,1)} %reshape.329), calls=%async_computation.4 | async-start | bytes 1048576 | tf_op jit(solution)/shard_map/all_to_all | solution.py:146
  328.0 15.3 %copy-start.29 = (f32[2048]{0:T(1024)S(1)}, f32[2048]{0:T(1024)}, u32[]{:S(2)}) copy-start(f32[2048]{0:T(1024)} %param.32) | copy-start | bytes 24580
  343.7 4.8 copy-start.30
  357.2 97.4 %copy-start.33 = (bf16[1,2048,1024]{2,1,0:T(8,128)(2,1)S(1)}, bf16[1,2048,1024]{2,1,0:T(8,128)(2,1)}, u32[]{:S(2)}) copy-start(bf16[1,2048,1024]{2,1,0:T(8,128)(2,1)} %param.37) | copy-start | bytes 12582916
  454.6 4.5 copy-start.34
  459.2 5.7 copy-start.35
  491.0 4.1 copy-start.32
  491.0 98.3 %all-to-all-start.6 = ((bf16[32,1,1,32,2048]{4,3,2,1,0:T(8,128)(2,1)}), bf16[32,1,1,32,2048]{4,3,2,1,0:T(8,128)(2,1)}, u32[]{:S(2)}, u32[]{:S(2)}) async-start(bf16[32,1,1,32,2048]{4,3,2,1,0:T(8,128)(2,1)} %fusion.76), calls=%async_computation.6 | async-start | bytes 8388608 | tf_op jit(solution)/shard_map/all_to_all | solution.py:192
Sparse Core Ops, SparseCore 0:
  18.9 59.6 all-gather.1
